TPU v7x, 32 devices: a whole 2x2x4 slice. The times are simulated.
32 devices in a mesh: gr: 2 (over x), fs: 8 (over z, y), tp: 2 (over core).
Axes of the slice: x: 2, y: 2, z: 4, core: 2. Of those that a mesh axis runs over, the one named last changes fastest.
Arguments:
- prompt: bfloat16 [3072, 2048], P(('gr', 'fs', 'tp')), may hold values from -6 to 6
- norm_first: float32 [2048], P(('gr', 'fs')), may hold values from 0.1 to 1.9
- gate_first: float32 [2048, 5632], P(('gr', 'fs'), 'tp'), may hold values from -6 to 6
- up_first: float32 [2048, 5632], P(('gr', 'fs'), 'tp'), may hold values from -6 to 6
- down_first: float32 [2048, 5632], P(('gr', 'fs'), 'tp'), may hold values from -6 to 6
- norm_second: float32 [2048], P(('gr', 'fs')), may hold values from 0.1 to 1.9
- gate_second: float32 [2048, 5632], P(('gr', 'fs'), 'tp'), may hold values from -6 to 6
- up_second: float32 [2048, 5632], P(('gr', 'fs'), 'tp'), may hold values from -6 to 6
- down_second: float32 [2048, 5632], P(('gr', 'fs'), 'tp'), may hold values from -6 to 6
Outputs:
- served_gate_first: bfloat16 [2048, 5632], P(None, 'fs')
- served_up_first: bfloat16 [2048, 5632], P(None, 'fs')
- served_down_first: bfloat16 [2048, 5632], P(None, 'fs')
- served_gate_second: bfloat16 [2048, 5632], P(None, 'fs')
- served_up_second: bfloat16 [2048, 5632], P(None, 'fs')
- served_down_second: bfloat16 [2048, 5632], P(None, 'fs')
- result: bfloat16 [3072, 2048], P(('gr', 'fs', 'tp'))
All inputs are finite; a program needn't handle non-finite values.
Results may differ from a plain program's by a relative error of at most 0.015.
Values may be sent and summed in bfloat16 or wider, within the bound.
A program may use at most 128 MiB of HBM per device.

v0:
```python
import jax
import jax.numpy as jnp
from jax import lax
from jax.sharding import PartitionSpec as P

D = 2048
FF = 5632
EPS = 1e-06


def fold_rows(gain, weight):
    return (gain[:, None] * weight).astype(jnp.bfloat16)


def relayout(stacked):
    moved = lax.all_to_all(
        lax.all_to_all(stacked, "tp", split_axis=1, concat_axis=2, tiled=True),
        "fs",
        split_axis=2,
        concat_axis=1,
        tiled=True,
    )
    whole = lax.all_gather(moved, ("gr", "tp"), axis=1, tiled=True)
    matrices = stacked.shape[0]
    block_width = moved.shape[2]
    gr_size = lax.axis_size("gr")
    tp_size = lax.axis_size("tp")
    fs_size = lax.axis_size("fs")
    sub_rows = stacked.shape[1] // tp_size
    shaped = whole.reshape(matrices, gr_size, tp_size, fs_size, sub_rows, block_width)
    return shaped.transpose(0, 1, 3, 2, 4, 5).reshape(
        matrices, gr_size * fs_size * tp_size * sub_rows, block_width
    )


def half_step(residual, weights):
    gate_weight = weights[0]
    up_weight = weights[1]
    down_weight = weights[2]
    resid_f = residual.astype(jnp.float32)
    normed = (
        resid_f * lax.rsqrt(jnp.mean(resid_f * resid_f, axis=-1, keepdims=True) + EPS)
    ).astype(jnp.bfloat16)
    in_scale = D ** (-0.5)
    out_scale = FF ** (-0.5)
    tokens_in = lax.all_gather(normed, "fs", axis=0, tiled=True)
    gate_pre = jnp.dot(tokens_in, gate_weight, preferred_element_type=jnp.float32) * in_scale
    up_pre = jnp.dot(tokens_in, up_weight, preferred_element_type=jnp.float32) * in_scale
    hidden = (jax.nn.silu(gate_pre) * up_pre).astype(jnp.bfloat16)
    branch = lax.psum_scatter(
        (
            lax.dot_general(
                hidden, down_weight, (((1,), (1,)), ((), ())), preferred_element_type=jnp.float32
            )
            * out_scale
        ).astype(jnp.bfloat16),
        "fs",
        scatter_dimension=0,
        tiled=True,
    ).astype(jnp.float32)
    return (resid_f + 0.5 * branch).astype(jnp.bfloat16)


def on_device(
    prompt,
    norm_first,
    gate_first,
    up_first,
    down_first,
    norm_second,
    gate_second,
    up_second,
    down_second,
):
    first_set = jnp.stack(
        [
            fold_rows(norm_first, gate_first),
            fold_rows(norm_first, up_first),
            down_first.astype(jnp.bfloat16),
        ]
    )
    second_set = jnp.stack(
        [
            fold_rows(norm_second, gate_second),
            fold_rows(norm_second, up_second),
            down_second.astype(jnp.bfloat16),
        ]
    )
    served_first = relayout(first_set)
    middle = half_step(prompt, served_first)
    served_second = relayout(second_set)
    result = half_step(middle, served_second)
    return (
        served_first[0],
        served_first[1],
        served_first[2],
        served_second[0],
        served_second[1],
        served_second[2],
        result,
    )


def solution(mesh):
    in_specs = (
        P(("gr", "fs", "tp"), None),
        P(("gr", "fs")),
        P(("gr", "fs"), "tp"),
        P(("gr", "fs"), "tp"),
        P(("gr", "fs"), "tp"),
        P(("gr", "fs")),
        P(("gr", "fs"), "tp"),
        P(("gr", "fs"), "tp"),
        P(("gr", "fs"), "tp"),
    )
    out_specs = (
        P(None, "fs"),
        P(None, "fs"),
        P(None, "fs"),
        P(None, "fs"),
        P(None, "fs"),
        P(None, "fs"),
        P(("gr", "fs", "tp"), None),
    )
    return jax.shard_map(
        on_device, mesh=mesh, in_specs=in_specs, out_specs=out_specs, check_vma=False
    )
```

profile of v0, /device:TPU:0, one launch (start us, length us, event | category | flops | bytes accessed | tf_op | source)
XLA Modules:
  0.0 607.6 jit_solution(7273351563624397723)
XLA Ops:
  7.2 2.5 fusion.6
  9.7 0.2 pad_maximum_fusion
  10.0 1.9 copy.52
  11.8 6.0 all_to_all.72
  17.9 2.6 copy.77
  20.5 10.8 %copy.72 = bf16[3,64,2,2816]{1,0,3,2:T(4,128)(2,1)} copy(bf16[3,64,2,2816]{3,2,1,0:T(2,128)(2,1)S(1)} %bitcast.78) | data formatting | bytes 4325376 | tf_op jit(solution)/shard_map/all_to_all | solution.py:17
  31.3 7.1 %reshape.54 = bf16[8,2,67584]{2,1,0:T(2,128)(2,1)S(1)} reshape(bf16[5632,3,64]{2,1,0:T(4,128)(2,1)} %bitcast.56) | data formatting | bytes 4325376
  38.4 57.7 %all_to_all.73 = bf16[8,2,67584]{2,1,0:T(2,128)(2,1)} all-to-all(bf16[8,2,67584]{2,1,0:T(2,128)(2,1)S(1)} %reshape.54), channel_id=1, replica_groups=mesh['gr'=2,'fs'=8,'tp'=2] {'fs'}, dimensions={0} | all-to-all | bytes 4325376 | tf_op jit(solution)/shard_map/all_to_all | solution.py:16
  96.1 8.0 %reshape.55 = bf16[5632,3,64]{2,1,0:T(4,128)(2,1)} reshape(bf16[8,2,67584]{2,1,0:T(2,128)(2,1)} %all_to_all.73) | data formatting | bytes 4325376
  104.1 9.4 %copy.55 = bf16[3,64,8,704]{3,1,2,0:T(8,128)(2,1)} copy(bf16[3,64,8,704]{1,0,3,2:T(4,128)(2,1)} %bitcast.57) | data formatting | bytes 4325376 | tf_op jit(solution)/shard_map/all_to_all | solution.py:16
  113.8 0.9 fusion.1
  114.7 0.3 reduce-scatter.3.cloned.1.call-start
  115.0 61.3 %all-gather.5.cloned.1.call-done = bf16[3,2048,704]{2,1,0:T(8,128)(2,1)} async-done(((bf16[3,512,704]{2,1,0:T(8,128)(2,1)}), bf16[3,2048,704]{2,1,0:T(8,128)(2,1)}) %all-gather.5.cloned.1.call-update) | async-done | bytes 8650768 | tf_op jit(solution)/shard_map/all_gather | solution.py:23
  176.3 4.1 fusion.15
  180.4 0.3 copy.56
  180.8 1.9 copy.57
  182.6 1.8 copy.58
  184.5 54.6 %all-gather.9.cloned.1.call-done = bf16[768,2048]{1,0:T(8,128)(2,1)} async-done(((bf16[96,2048]{1,0:T(8,128)(2,1)}), bf16[768,2048]{1,0:T(8,128)(2,1)}) %all-gather.9.cloned.1.call-update) | async-done | bytes 3145744 | tf_op jit(solution)/shard_map/all_gather | solution.py:46
  239.1 5.7 fusion.16
  244.8 12.4 %multiply_convert_fusion.1 = bf16[768,2048]{1,0:T(8,128)(2,1)} fusion(bf16[2048,704]{1,0:T(8,128)(2,1)} %bitcast.64, f32[768,704]{0,1:T(8,128)} %fusion.16, bf16[768,2048]{1,0:T(8,128)(2,1)} %all-gather.9.cloned.1.call-done, bf16[2048,704]{1,0:T(8,128)(2,1)} %bitcast.62), kind=kOutput, calls=%fused_computation.1 | convolution fusion | flops 4436656128 | bytes 14221312 | tf_op jit(solution)/shard_map/dot_general | solution.py:52
  257.3 0.5 all-gather.7.cloned.1.call-start
  257.9 2.5 fusion.8
  260.6 1.9 copy.59
  262.5 6.0 all_to_all.74
  268.5 3.9 copy.76
  272.5 15.1 %copy.73 = bf16[3,64,2,2816]{1,0,3,2:T(4,128)(2,1)} copy(bf16[3,64,2,2816]{3,2,1,0:T(2,128)(2,1)} %bitcast.79) | data formatting | bytes 4325376 | tf_op jit(solution)/shard_map/all_to_all | solution.py:17
  287.6 8.2 %reshape.56 = bf16[8,2,67584]{2,1,0:T(2,128)(2,1)} reshape(bf16[5632,3,64]{2,1,0:T(4,128)(2,1)} %bitcast.58) | data formatting | bytes 4325376
  295.9 67.8 %all_to_all.75 = bf16[8,2,67584]{2,1,0:T(2,128)(2,1)} all-to-all(bf16[8,2,67584]{2,1,0:T(2,128)(2,1)} %reshape.56), channel_id=1, replica_groups=mesh['gr'=2,'fs'=8,'tp'=2] {'fs'}, dimensions={0} | all-to-all | bytes 4325376 | tf_op jit(solution)/shard_map/all_to_all | solution.py:16
  363.7 8.0 %reshape.57 = bf16[5632,3,64]{2,1,0:T(4,128)(2,1)} reshape(bf16[8,2,67584]{2,1,0:T(2,128)(2,1)} %all_to_all.75) | data formatting | bytes 4325376
  371.6 9.4 %copy.62 = bf16[3,64,8,704]{3,1,2,0:T(8,128)(2,1)} copy(bf16[3,64,8,704]{1,0,3,2:T(4,128)(2,1)} %bitcast.59) | data formatting | bytes 4325376 | tf_op jit(solution)/shard_map/all_to_all | solution.py:16
  381.1 1.3 fusion.3
  382.4 1.9 fusion.4
  384.5 59.3 %all-gather.7.cloned.1.call-done = bf16[3,2048,704]{2,1,0:T(8,128)(2,1)} async-done(((bf16[3,512,704]{2,1,0:T(8,128)(2,1)}), bf16[3,2048,704]{2,1,0:T(8,128)(2,1)}) %all-gather.7.cloned.1.call-update) | async-done | bytes 8650768 | tf_op jit(solution)/shard_map/all_gather | solution.py:23
  443.8 4.1 fusion.14
  447.9 1.9 copy.63
  449.8 1.9 copy.64
  451.7 1.9 copy.65
  453.6 52.8 %all-gather.11.cloned.1.call-done = bf16[768,2048]{1,0:T(8,128)(2,1)} async-done(((bf16[96,2048]{1,0:T(8,128)(2,1)}), bf16[768,2048]{1,0:T(8,128)(2,1)}) %all-gather.11.cloned.1.call-update) | async-done | bytes 3145744 | tf_op jit(solution)/shard_map/all_gather | solution.py:46
  506.5 6.6 %fusion.17 = f32[768,704]{0,1:T(8,128)} fusion(bf16[768,2048]{1,0:T(8,128)(2,1)} %all-gather.11.cloned.1.call-done, bf16[2048,704]{1,0:T(8,128)(2,1)} %bitcast.66), kind=kOutput, calls=%fused_computation.39 | convolution fusion | flops 2214592512 | bytes 8192000 | tf_op jit(solution)/shard_map/dot_general | solution.py:47
  513.1 12.4 %multiply_convert_fusion = bf16[768,2048]{1,0:T(8,128)(2,1)} fusion(bf16[2048,704]{1,0:T(8,128)(2,1)} %bitcast.70, f32[768,704]{0,1:T(8,128)} %fusion.17, bf16[768,2048]{1,0:T(8,128)(2,1)} %all-gather.11.cloned.1.call-done, bf16[2048,704]{1,0:T(8,128)(2,1)} %bitcast.68), kind=kOutput, calls=%fused_computation | convolution fusion | flops 4436656128 | bytes 14221312 | tf_op jit(solution)/shard_map/dot_general | solution.py:52
  525.6 4.6 copy.69
  530.1 4.6 copy.70
  534.7 4.6 copy.71
  539.2 2.7 copy.66
  541.9 4.7 copy.67
  546.7 2.7 copy.68
  549.3 49.1 %reduce-scatter.5.cloned.1.call-done = bf16[96,2048]{1,0:T(8,128)(2,1)} async-done(((bf16[768,2048]{1,0:T(8,128)(2,1)}), bf16[96,2048]{1,0:T(8,128)(2,1)}) %reduce-scatter.5.cloned.1.call-update) | async-done | bytes 393232 | tf_op jit(solution)/shard_map/reduce_scatter | solution.py:50
  598.5 2.1 fusion.5
  (21 shorter events, 1.0 us)
Async XLA Ops:
  7.2 169.1 %all-gather.5.cloned.1.call-start = ((), (), s32[]{:S(2)}) async-start(), calls=%async_computation.6 | async-start | bytes 11796480 | tf_op jit(solution)/shard_map/all_gather | solution.py:23
  104.1 9.5 %copy-start.1 = (bf16[96,2048]{1,0:T(8,128)(2,1)S(1)}, bf16[96,2048]{1,0:T(8,128)(2,1)}, u32[]{:S(2)}) copy-start(bf16[96,2048]{1,0:T(8,128)(2,1)} %param.9) | copy-start | bytes 1179652
  113.5 125.6 %all-gather.9.cloned.1.call-start = ((), (), s32[]{:S(2)}) async-start(), calls=%async_computation.8 | async-start | bytes 3538944 | tf_op jit(solution)/shard_map/all_gather | solution.py:46
  114.7 266.4 %reduce-scatter.3.cloned.1.call-start = ((), (), s32[]{:S(2)}) async-start(), calls=%async_computation.9 | async-start | bytes 3538944 | tf_op jit(solution)/shard_map/reduce_scatter | solution.py:50
  257.2 0.7 copy-start.2
  257.3 186.5 %all-gather.7.cloned.1.call-start = ((), (), s32[]{:S(2)}) async-start(), calls=%async_computation.7 | async-start | bytes 11796480 | tf_op jit(solution)/shard_map/all_gather | solution.py:23
  381.0 125.4 %all-gather.11.cloned.1.call-start = ((), (), s32[]{:S(2)}) async-start(), calls=%async_computation.10 | async-start | bytes 3538944 | tf_op jit(solution)/shard_map/all_gather | solution.py:46
  384.3 214.2 %reduce-scatter.5.cloned.1.call-start = ((), (), s32[]{:S(2)}) async-start(), calls=%async_computation.11 | async-start | bytes 3538944 | tf_op jit(solution)/shard_map/reduce_scatter | solution.py:50
  541.9 4.7 copy-start
Sparse Core Ops, SparseCore 0:
  113.6 62.6 all-gather.4
  179.1 60.0 all-gather.8
  257.4 96.6 reduce-scatter.2
  381.2 62.5 all-gather.6
  446.4 60.0 all-gather.10
  525.7 72.7 reduce-scatter.4
where the time goes:
time: 615 us; the launch traced here: 608 us
  waiting for transfers between devices  277 us (45%)
  blocking collectives  138 us (22%)
  local copies, waits for them, and re-layouts  128 us (21%)
  matrix products  37.2 us (6%)
  between operations  14.4 us (2%)
  other arithmetic  11.8 us (2%)
    all_to_all x2, blocking collectives, relayout(): lax.all_to_all(lax.all_to_all(stacked, 'tp', split_axis=1, concat_axis=2,...  126 us
    all_gather x2, waiting for transfers between devices, relayout(): whole = lax.all_gather(moved, ('gr', 'tp'), axis=1, tiled=True)  121 us
    all_gather x2, waiting for transfers between devices, half_step(): tokens_in = lax.all_gather(normed, 'fs', axis=0, tiled=True)  107 us
    unnamed x16, local copies, waits for them, and re-layouts  55.2 us
    reduce_scatter x2, waiting for transfers between devices, half_step(): lax.psum_scatter((lax.dot_general(hidden, down_weight, (((1,), (1,)), (()...  49.1 us
    all_to_all x4, local copies, waits for them, and re-layouts, relayout(): lax.all_to_all(stacked, 'tp', split_axis=1, concat_axis=2, tiled=True)  32.4 us
    dot_general x2, matrix products, half_step(): lax.dot_general(hidden, down_weight, (((1,), (1,)), ((), ())), preferred_...  24.9 us
    all_to_all x2, local copies, waits for them, and re-layouts, relayout(): lax.all_to_all(lax.all_to_all(stacked, 'tp', split_axis=1, concat_axis=2,...  18.8 us
  transfers between devices with their start and end apart: 6, of which 5 were waited for; matrix products, arithmetic and copies ran while one was open for 16% of the time, Pallas kernels for 0%

commit v1 on v0

--- a/solution.py
+++ b/solution.py
@@ -8,18 +8,25 @@
 EPS = 1e-06
 
 
+def row_wrap(dim_k, at_axis, here_x):
+    e_now = jnp.concatenate(
+        jax.lax.all_to_all(
+            jnp.stack(jnp.split(here_x, jax.lax.axis_size("tp"), axis=at_axis), axis=0),
+            "tp",
+            concat_axis=0,
+            split_axis=0,
+        ),
+        axis=dim_k,
+    )
+    return e_now
+
+
 def fold_rows(gain, weight):
     return (gain[:, None] * weight).astype(jnp.bfloat16)
 
 
 def relayout(stacked):
-    moved = lax.all_to_all(
-        lax.all_to_all(stacked, "tp", split_axis=1, concat_axis=2, tiled=True),
-        "fs",
-        split_axis=2,
-        concat_axis=1,
-        tiled=True,
-    )
+    moved = lax.all_to_all(row_wrap(2, 1, stacked), "fs", split_axis=2, concat_axis=1, tiled=True)
     whole = lax.all_gather(moved, ("gr", "tp"), axis=1, tiled=True)
     matrices = stacked.shape[0]
     block_width = moved.shape[2]

time: 615 us -> 589 us (0.958)
  local copies, waits for them, and re-layouts: 128 us -> 108 us
    all_to_all x6 -> x2, local copies, waits for them, and re-layouts: 51.2 us -> 18.7 us  [relayout(): lax.all_to_all(row_wrap(2, 1, stacked), 'fs', split_axis=2, concat_axis=1...]
    reshape x0 -> x2, local copies, waits for them, and re-layouts: none -> 14.8 us  [row_wrap(): jnp.concatenate(jax.lax.all_to_all(jnp.stack(jnp.split(here_x, jax.lax.ax...]
  transfers between devices with their start and end apart: 6 -> 6, of which waited for: 5 -> 5; matrix products, arithmetic and copies ran while one was open for 16% -> 14% of each run, Pallas kernels for 0% -> 0%
where the time goes in v1:
time: 589 us; the launch traced here: 587 us
  waiting for transfers between devices  277 us (47%)
  blocking collectives  137 us (23%)
  local copies, waits for them, and re-layouts  108 us (18%)
  matrix products  37.2 us (6%)
  between operations  14.2 us (2%)
  other arithmetic  12.2 us (2%)
    all_to_all x2, blocking collectives, relayout(): lax.all_to_all(row_wrap(2, 1, stacked), 'fs', split_axis=2, concat_axis=1...  126 us
    all_gather x2, waiting for transfers between devices, relayout(): whole = lax.all_gather(moved, ('gr', 'tp'), axis=1, tiled=True)  120 us
    all_gather x2, waiting for transfers between devices, half_step(): tokens_in = lax.all_gather(normed, 'fs', axis=0, tiled=True)  107 us
    unnamed x16, local copies, waits for them, and re-layouts  56.6 us
    reduce_scatter x2, waiting for transfers between devices, half_step(): lax.psum_scatter((lax.dot_general(hidden, down_weight, (((1,), (1,)), (()...  49.1 us
    dot_general x2, matrix products, half_step(): lax.dot_general(hidden, down_weight, (((1,), (1,)), ((), ())), preferred_...  24.9 us
    all_to_all x2, local copies, waits for them, and re-layouts, relayout(): lax.all_to_all(row_wrap(2, 1, stacked), 'fs', split_axis=2, concat_axis=1...  18.7 us
    reshape x2, local copies, waits for them, and re-layouts, row_wrap(): jnp.concatenate(jax.lax.all_to_all(jnp.stack(jnp.split(here_x, jax.lax.ax...  14.8 us
  transfers between devices with their start and end apart: 6, of which 5 were waited for; matrix products, arithmetic and copies ran while one was open for 14% of the time, Pallas kernels for 0%

profile of v1, /device:TPU:0, one launch (start us, length us, event | category | flops | bytes accessed | tf_op | source)
XLA Modules:
  0.0 586.6 jit_solution(13249659042891682077)
XLA Ops:
  7.2 2.5 fusion.6
  9.7 0.2 pad_maximum_fusion
  10.3 5.5 all_to_all.46
  15.8 6.2 %copy.50 = bf16[3,64,2,2816]{1,0,3,2:T(4,128)(2,1)} copy(bf16[3,64,2,2816]{3,1,0,2:T(8,128)(2,1)S(1)} %bitcast.78) | data formatting | bytes 4325376 | tf_op jit(solution)/shard_map/reshape | solution.py:12
  22.0 7.1 %reshape.70 = bf16[8,2,67584]{2,1,0:T(2,128)(2,1)S(1)} reshape(bf16[5632,3,64]{2,1,0:T(4,128)(2,1)} %bitcast.58) | data formatting | bytes 4325376
  29.1 57.7 %all_to_all.47 = bf16[8,2,67584]{2,1,0:T(2,128)(2,1)} all-to-all(bf16[8,2,67584]{2,1,0:T(2,128)(2,1)S(1)} %reshape.70), channel_id=1, replica_groups=mesh['gr'=2,'fs'=8,'tp'=2] {'fs'}, dimensions={0} | all-to-all | bytes 4325376 | tf_op jit(solution)/shard_map/all_to_all | solution.py:29
  86.9 8.0 %reshape.71 = bf16[5632,3,64]{2,1,0:T(4,128)(2,1)} reshape(bf16[8,2,67584]{2,1,0:T(2,128)(2,1)} %all_to_all.47) | data formatting | bytes 4325376
  94.8 9.4 %copy.34 = bf16[3,64,8,704]{3,1,2,0:T(8,128)(2,1)} copy(bf16[3,64,8,704]{1,0,3,2:T(4,128)(2,1)} %bitcast.59) | data formatting | bytes 4325376 | tf_op jit(solution)/shard_map/all_to_all | solution.py:29
  104.3 0.9 copy-done.1
  105.4 0.9 fusion.1
  106.3 0.2 reduce-scatter.3.cloned.1.call-start
  106.5 60.5 %all-gather.5.cloned.1.call-done = bf16[3,2048,704]{2,1,0:T(8,128)(2,1)} async-done(((bf16[3,512,704]{2,1,0:T(8,128)(2,1)}), bf16[3,2048,704]{2,1,0:T(8,128)(2,1)}) %all-gather.5.cloned.1.call-update) | async-done | bytes 8650768 | tf_op jit(solution)/shard_map/all_gather | solution.py:30
  167.0 4.1 fusion.15
  171.1 0.3 copy.35
  171.5 1.9 copy.36
  173.3 1.9 copy.37
  175.2 54.6 %all-gather.9.cloned.1.call-done = bf16[768,2048]{1,0:T(8,128)(2,1)} async-done(((bf16[96,2048]{1,0:T(8,128)(2,1)}), bf16[768,2048]{1,0:T(8,128)(2,1)}) %all-gather.9.cloned.1.call-update) | async-done | bytes 3145744 | tf_op jit(solution)/shard_map/all_gather | solution.py:53
  229.8 5.7 fusion.16
  235.5 12.4 %multiply_convert_fusion.1 = bf16[768,2048]{1,0:T(8,128)(2,1)} fusion(bf16[2048,704]{1,0:T(8,128)(2,1)} %bitcast.66, f32[768,704]{0,1:T(8,128)} %fusion.16, bf16[768,2048]{1,0:T(8,128)(2,1)} %all-gather.9.cloned.1.call-done, bf16[2048,704]{1,0:T(8,128)(2,1)} %bitcast.64), kind=kOutput, calls=%fused_computation.1 | convolution fusion | flops 4436656128 | bytes 14221312 | tf_op jit(solution)/shard_map/dot_general | solution.py:59
  248.0 0.6 copy-done.2
  248.6 2.5 fusion.8
  251.1 0.2 pad_maximum_fusion.2
  251.5 0.2 pad_maximum_fusion.3
  251.7 6.4 %all_to_all.48 = bf16[2,3,64,2816]{3,2,1,0:T(8,128)(2,1)} all-to-all(bf16[2,3,64,2816]{3,2,1,0:T(8,128)(2,1)S(1)} %pad_maximum_fusion.3), channel_id=1, replica_groups=mesh['gr'=2,'fs'=8,'tp'=2] {'tp'}, dimensions={0} | all-to-all | bytes 4325376 | tf_op jit(solution)/shard_map/all_to_all | solution.py:13
  258.1 8.6 %copy.51 = bf16[3,64,2,2816]{1,0,3,2:T(4,128)(2,1)} copy(bf16[3,64,2,2816]{3,1,0,2:T(8,128)(2,1)} %bitcast.79) | data formatting | bytes 4325376 | tf_op jit(solution)/shard_map/reshape | solution.py:12
  266.6 8.3 %reshape.72 = bf16[8,2,67584]{2,1,0:T(2,128)(2,1)} reshape(bf16[5632,3,64]{2,1,0:T(4,128)(2,1)} %bitcast.60) | data formatting | bytes 4325376
  274.9 67.8 %all_to_all.49 = bf16[8,2,67584]{2,1,0:T(2,128)(2,1)} all-to-all(bf16[8,2,67584]{2,1,0:T(2,128)(2,1)} %reshape.72), channel_id=1, replica_groups=mesh['gr'=2,'fs'=8,'tp'=2] {'fs'}, dimensions={0} | all-to-all | bytes 4325376 | tf_op jit(solution)/shard_map/all_to_all | solution.py:29
  342.8 8.0 %reshape.73 = bf16[5632,3,64]{2,1,0:T(4,128)(2,1)} reshape(bf16[8,2,67584]{2,1,0:T(2,128)(2,1)} %all_to_all.49) | data formatting | bytes 4325376
  350.7 9.4 %copy.40 = bf16[3,64,8,704]{3,1,2,0:T(8,128)(2,1)} copy(bf16[3,64,8,704]{1,0,3,2:T(4,128)(2,1)} %bitcast.61) | data formatting | bytes 4325376 | tf_op jit(solution)/shard_map/all_to_all | solution.py:29
  360.2 1.3 fusion.3
  361.5 1.9 fusion.4
  363.4 0.3 reduce-scatter.5.cloned.1.call-start
  363.7 59.4 %all-gather.7.cloned.1.call-done = bf16[3,2048,704]{2,1,0:T(8,128)(2,1)} async-done(((bf16[3,512,704]{2,1,0:T(8,128)(2,1)}), bf16[3,2048,704]{2,1,0:T(8,128)(2,1)}) %all-gather.7.cloned.1.call-update) | async-done | bytes 8650768 | tf_op jit(solution)/shard_map/all_gather | solution.py:30
  423.1 4.1 fusion.14
  427.2 1.9 copy.41
  429.1 1.9 copy.42
  431.0 1.9 copy.43
  432.9 52.8 %all-gather.11.cloned.1.call-done = bf16[768,2048]{1,0:T(8,128)(2,1)} async-done(((bf16[96,2048]{1,0:T(8,128)(2,1)}), bf16[768,2048]{1,0:T(8,128)(2,1)}) %all-gather.11.cloned.1.call-update) | async-done | bytes 3145744 | tf_op jit(solution)/shard_map/all_gather | solution.py:53
  485.7 6.6 %fusion.17 = f32[768,704]{0,1:T(8,128)} fusion(bf16[768,2048]{1,0:T(8,128)(2,1)} %all-gather.11.cloned.1.call-done, bf16[2048,704]{1,0:T(8,128)(2,1)} %bitcast.68), kind=kOutput, calls=%fused_computation.43 | convolution fusion | flops 2214592512 | bytes 8192000 | tf_op jit(solution)/shard_map/dot_general | solution.py:54
  492.4 12.4 %multiply_convert_fusion = bf16[768,2048]{1,0:T(8,128)(2,1)} fusion(bf16[2048,704]{1,0:T(8,128)(2,1)} %bitcast.72, f32[768,704]{0,1:T(8,128)} %fusion.17, bf16[768,2048]{1,0:T(8,128)(2,1)} %all-gather.11.cloned.1.call-done, bf16[2048,704]{1,0:T(8,128)(2,1)} %bitcast.70), kind=kOutput, calls=%fused_computation | convolution fusion | flops 4436656128 | bytes 14221312 | tf_op jit(solution)/shard_map/dot_general | solution.py:59
  504.8 4.6 copy.47
  509.4 4.6 copy.48
  514.0 4.6 copy.49
  518.5 2.7 copy.44
  521.2 4.7 copy.45
  525.9 2.7 copy.46
  528.6 49.1 %reduce-scatter.5.cloned.1.call-done = bf16[96,2048]{1,0:T(8,128)(2,1)} async-done(((bf16[768,2048]{1,0:T(8,128)(2,1)}), bf16[96,2048]{1,0:T(8,128)(2,1)}) %reduce-scatter.5.cloned.1.call-update) | async-done | bytes 393232 | tf_op jit(solution)/shard_map/reduce_scatter | solution.py:57
  577.7 2.1 fusion.5
  (21 shorter events, 1.0 us)
Async XLA Ops:
  7.2 159.9 %all-gather.5.cloned.1.call-start = ((), (), s32[]{:S(2)}) async-start(), calls=%async_computation.6 | async-start | bytes 11796480 | tf_op jit(solution)/shard_map/all_gather | solution.py:30
  104.2 1.0 copy-start.1
  104.2 125.6 %all-gather.9.cloned.1.call-start = ((), (), s32[]{:S(2)}) async-start(), calls=%async_computation.8 | async-start | bytes 3538944 | tf_op jit(solution)/shard_map/all_gather | solution.py:53
  106.3 253.9 %reduce-scatter.3.cloned.1.call-start = ((), (), s32[]{:S(2)}) async-start(), calls=%async_computation.9 | async-start | bytes 3538944 | tf_op jit(solution)/shard_map/reduce_scatter | solution.py:57
  247.9 0.7 copy-start.2
  248.0 175.1 %all-gather.7.cloned.1.call-start = ((), (), s32[]{:S(2)}) async-start(), calls=%async_computation.7 | async-start | bytes 11796480 | tf_op jit(solution)/shard_map/all_gather | solution.py:30
  360.1 125.6 %all-gather.11.cloned.1.call-start = ((), (), s32[]{:S(2)}) async-start(), calls=%async_computation.10 | async-start | bytes 3538944 | tf_op jit(solution)/shard_map/all_gather | solution.py:53
  363.4 214.4 %reduce-scatter.5.cloned.1.call-start = ((), (), s32[]{:S(2)}) async-start(), calls=%async_computation.11 | async-start | bytes 3538944 | tf_op jit(solution)/shard_map/reduce_scatter | solution.py:57
  521.2 4.7 copy-start
Sparse Core Ops, SparseCore 0:
  104.4 62.6 all-gather.4
  169.8 60.0 all-gather.8
  248.1 92.2 reduce-scatter.2
  360.2 62.7 all-gather.6
  425.7 60.0 all-gather.10
  504.9 72.7 reduce-scatter.4
